TPU v7x, 32 devices: a whole 2x2x4 slice. The times are simulated.
32 devices in a mesh: sp: 4 (over z), dp: 8 (over y, x, core).
Axes of the slice: x: 2, y: 2, z: 4, core: 2. Of those that a mesh axis runs over, the one named last changes fastest.
Arguments:
- value_half: bfloat16 [8, 1536, 2048], P('dp', 'sp'), may hold values from -6 to 6
- gate_half: bfloat16 [8, 1536, 2048], P('dp', 'sp'), may hold values from -9 to 9
- conv_taps: bfloat16 [31, 2048], replicated, may hold values from -1 to 1
- norm_gain: float32 [2048], replicated, may hold values from 0.1 to 1.9
- norm_shift: float32 [2048], replicated, may hold values from -3 to 3
- out_weight: bfloat16 [2048, 2048], P('dp', 'sp'), may hold values from -0.125 to 0.125
Outputs:
- module_out: bfloat16 [8, 1536, 2048], P('dp', 'sp')
All inputs are finite; a program needn't handle non-finite values.
Results may differ from a plain program's by a relative error of at most 0.0064.
Values may be sent and summed in bfloat16 or wider, within the bound.
A program may use at most 64 MiB of HBM per device.

v0:
```python
import jax
import jax.numpy as jnp
from jax import lax
from jax.sharding import PartitionSpec as P

EPSILON = 1e-06


def passed_along(value, axis, steps):
    count = lax.axis_size(axis)
    initial, last = (max(0, -steps), min(count, count - steps))
    return lax.ppermute(value, axis, [(source, source + steps) for source in range(initial, last)])


def causal_mix(padded, conv_taps, length):
    tap_count = conv_taps.shape[0]
    running = jnp.zeros((length, padded.shape[1]), jnp.float32)
    for tap_index in range(tap_count):
        running = running + padded[tap_index : tap_index + length].astype(jnp.float32) * conv_taps[
            tap_index
        ].astype(jnp.float32)
    return running.astype(jnp.bfloat16)


def per_device(value_half, gate_half, conv_taps, norm_gain, norm_shift, out_weight):
    tap_count = conv_taps.shape[0]
    tok_rows = value_half.shape[1]
    gated = (
        value_half[0].astype(jnp.float32) * jax.nn.sigmoid(gate_half[0].astype(jnp.float32))
    ).astype(jnp.bfloat16)
    tail_rows = gated[tok_rows - (tap_count - 1) :]
    history = passed_along(tail_rows, "sp", 1)
    padded = jnp.concatenate([history, gated], 0)
    convolved = causal_mix(padded, conv_taps, tok_rows)
    widened = convolved.astype(jnp.float32)
    mean_row = jnp.mean(widened, axis=-1, keepdims=True)
    centered = widened - mean_row
    variance = jnp.mean(centered * centered, axis=-1, keepdims=True)
    normed = centered * lax.rsqrt(variance + EPSILON) * norm_gain + norm_shift
    activated = jax.nn.silu(normed).astype(jnp.bfloat16)
    row_block = lax.all_gather(out_weight, "sp", axis=1, tiled=True)
    projected = jnp.dot(
        activated,
        lax.all_gather(row_block, "dp", axis=0, tiled=True),
        preferred_element_type=jnp.float32,
    )
    return projected.astype(jnp.bfloat16)[None]


def solution(mesh):
    placed = (P("dp", "sp", None), P("dp", "sp", None), P(), P(), P(), P("dp", "sp"))
    return jax.shard_map(
        per_device, mesh=mesh, in_specs=placed, out_specs=P("dp", "sp", None), check_vma=False
    )
```

profile of v0, /device:TPU:17, one launch (start us, length us, event | category | flops | bytes accessed | tf_op | source)
XLA Modules:
  0.0 109.3 jit_solution(4330929815768049006)
XLA Ops:
  6.5 0.0 copy-start
  6.5 0.0 all-gather.3.cloned.1.call-start
  6.5 0.7 all-gather.3.cloned.1.call-update
  7.3 0.0 all-gather.5.cloned.1.call-start
  7.3 29.6 %all-gather.3.cloned.1.call-done = bf16[256,2048]{1,0:T(8,128)(2,1)} async-done(((bf16[256,512]{1,0:T(8,128)(2,1)}), bf16[256,2048]{1,0:T(8,128)(2,1)}) %all-gather.3.cloned.1.call-update) | async-done | bytes 1048592 | tf_op jit(solution)/shard_map/all_gather | solution.py:41
  36.9 0.0 all-gather.5.cloned.1.call-update
  36.9 2.8 %multiply_convert_fusion = bf16[1,384,2048]{2,1,0:T(8,128)(2,1)S(1)} fusion(bf16[1,384,2048]{2,1,0:T(8,128)(2,1)} %param.6, bf16[1,384,2048]{2,1,0:T(8,128)(2,1)} %param.7), kind=kLoop, calls=%fused_computation.42 | loop fusion | flops 5505024 | bytes 4718592 | tf_op jit(solution)/shard_map/convert_element_type | solution.py:30
  39.7 0.0 copy-start.1
  39.7 0.0 copy-start.2
  39.8 2.5 %collective-permute-start = (bf16[30,2048]{1,0:T(8,128)(2,1)S(1)}, bf16[30,2048]{1,0:T(8,128)(2,1)S(1)}, u32[]{:S(2)}, u32[]{:S(2)}) collective-permute-start(bf16[30,2048]{1,0:T(8,128)(2,1)S(1)} %slice_bitcast_fusion), channel_id=1, source_target_pairs={{0,8},{8,16},{16,24},{1,9},{9,17},{17,25},{2,10},{10,18},{18,26},{... | collective-permute-start | bytes 368648 | tf_op jit(solution)/shard_map/ppermute | solution.py:12
  42.3 0.0 copy-done
  42.3 0.1 slice_convert_fusion.30
  42.5 0.1 slice_convert_fusion.29
  42.5 3.0 %collective-permute-done = bf16[30,2048]{1,0:T(8,128)(2,1)S(1)} collective-permute-done((bf16[30,2048]{1,0:T(8,128)(2,1)S(1)}, bf16[30,2048]{1,0:T(8,128)(2,1)S(1)}, u32[]{:S(2)}, u32[]{:S(2)}) %collective-permute-start) | collective-permute-done | bytes 122912 | tf_op jit(solution)/shard_map/ppermute | solution.py:12
  45.5 14.3 %convert_reduce_fusion = (f32[384]{0:T(512)S(1)}, bf16[384,2048]{1,0:T(8,128)(2,1)S(1)}) fusion(f32[2048]{0:T(1024)S(1)} %bitcast.67, bf16[384,2048]{1,0:T(8,128)(2,1)S(1)} %bitcast.37, f32[2048]{0:T(1024)S(1)} %bitcast.68, bf16[30,2048]{1,0:T(8,128)(2,1)S(1)} %collective-permute-done, f32[2048]{0:T(1024)S(1)} %bitcast.39, f32[2048]{0:T(1024)S(1)} %bitcast.40, ...), kind=kLoop, calls=%fused_computation.30 | loop fusion | flops 145489536 | bytes 3524096 | tf_op jit(solution)/shard_map/reduce_sum | solution.py:36
  59.8 0.6 fusion.2
  60.4 33.6 %all-gather.5.cloned.1.call-done = bf16[2048,2048]{1,0:T(8,128)(2,1)} async-done(((bf16[256,2048]{1,0:T(8,128)(2,1)}), bf16[2048,2048]{1,0:T(8,128)(2,1)}) %all-gather.5.cloned.1.call-update) | async-done | bytes 8388624 | tf_op jit(solution)/shard_map/all_gather | solution.py:44
  94.0 0.0 copy-done.1
  94.0 0.0 copy-done.2
  94.0 8.5 %fusion.11 = bf16[1,384,2048]{2,1,0:T(8,128)(2,1)} fusion(bf16[2048,2048]{1,0:T(8,128)(2,1)} %all-gather.5.cloned.1.call-done, bf16[384,2048]{1,0:T(8,128)(2,1)S(1)} %get-tuple-element.6, f32[2048]{0:T(1024)S(1)} %copy-done.1, f32[2048]{0:T(1024)S(1)} %copy-done.2, f32[384]{0:T(512)S(1)} %add_rsqrt_fusion, f32[384]{0:T(512)S(1)} %broadcast_multiply_fusion), kind=kOutput, calls=%fused_computation.45 | convolution fusion | flops 3229876224 | bytes 11553792 | tf_op jit(solution)/shard_map/dot_general | solution.py:42
  (3 shorter events, 0.0 us)
Async XLA Ops:
  6.5 35.8 %copy-start = (bf16[31,2048]{1,0:T(8,128)(2,1)S(1)}, bf16[31,2048]{1,0:T(8,128)(2,1)}, u32[]{:S(2)}) copy-start(bf16[31,2048]{1,0:T(8,128)(2,1)} %param.8) | copy-start | bytes 380932
  6.5 30.4 %all-gather.3.cloned.1.call-start = ((), (), s32[]{:S(2)}) async-start(), calls=%async_computation | async-start | bytes 1310720 | tf_op jit(solution)/shard_map/all_gather | solution.py:41
  7.3 86.7 %all-gather.5.cloned.1.call-start = ((), (), s32[]{:S(2)}) async-start(), calls=%async_computation.1 | async-start | bytes 9437184 | tf_op jit(solution)/shard_map/all_gather | solution.py:44
  39.7 54.2 %copy-start.1 = (f32[2048]{0:T(1024)S(1)}, f32[2048]{0:T(1024)}, u32[]{:S(2)}) copy-start(f32[2048]{0:T(1024)} %param.10) | copy-start | bytes 24580
  39.7 54.2 %copy-start.2 = (f32[2048]{0:T(1024)S(1)}, f32[2048]{0:T(1024)}, u32[]{:S(2)}) copy-start(f32[2048]{0:T(1024)} %param.9) | copy-start | bytes 24580
  39.8 5.7 %collective-permute-start = (bf16[30,2048]{1,0:T(8,128)(2,1)S(1)}, bf16[30,2048]{1,0:T(8,128)(2,1)S(1)}, u32[]{:S(2)}, u32[]{:S(2)}) collective-permute-start(bf16[30,2048]{1,0:T(8,128)(2,1)S(1)} %slice_bitcast_fusion), channel_id=1, source_target_pairs={{0,8},{8,16},{16,24},{1,9},{9,17},{17,25},{2,10},{10,18},{18,26},{... | collective-permute-start | bytes 368648 | tf_op jit(solution)/shard_map/ppermute | solution.py:12
Sparse Core Ops, SparseCore 0:
  8.9 27.9 all-gather.2
  38.8 55.1 all-gather.4
where the time goes:
time: 111 us; the launch traced here: 109 us
  waiting for transfers between devices  66.9 us (60%)
  other arithmetic  17.8 us (16%)
  between operations  13.5 us (12%)
  matrix products  8.49 us (8%)
  starting transfers between devices  2.56 us (2%)
    all_gather x1, waiting for transfers between devices, per_device(): lax.all_gather(row_block, 'dp', axis=0, tiled=True)  33.6 us
    all_gather x1, waiting for transfers between devices, per_device(): row_block = lax.all_gather(out_weight, 'sp', axis=1, tiled=True)  29.6 us
    reduce_sum x1, other arithmetic, per_device(): mean_row = jnp.mean(widened, axis=-1, keepdims=True)  14.3 us
    dot_general x1, matrix products, per_device(): jnp.dot(activated, lax.all_gather(row_block, 'dp', axis=0, tiled=True), p...  8.49 us
    ppermute x1, waiting for transfers between devices, passed_along(): lax.ppermute(value, axis, [(source, source + steps) for source in range(i...  2.98 us
    convert_element_type x1, other arithmetic, per_device(): gated = (value_half[0].astype(jnp.float32) * jax.nn.sigmoid(gate_half[0]....  2.79 us
    ppermute x1, starting transfers between devices, passed_along(): lax.ppermute(value, axis, [(source, source + steps) for source in range(i...  2.52 us
  transfers between devices with their start and end apart: 3, of which 3 were waited for; matrix products, arithmetic and copies ran while one was open for 16% of the time, Pallas kernels for 0%

commit v1 on v0

v1 whole, which is shorter than its diff:
```python
import math

import jax
import jax.numpy as jnp
from jax import lax
from jax.experimental import pallas as pl
from jax.experimental.pallas import tpu as pltpu
from jax.sharding import PartitionSpec as P

EPSILON = 1e-06
MESH = pl.DeviceIdType.MESH
F32 = jnp.float32
BF16 = jnp.bfloat16
LANES = 128


def half_sigmoid(x):
    return 0.5 * jnp.tanh(0.5 * x) + 0.5


def nearest(me, count, k):
    place = jnp.int32(0)
    for here in range(count):
        there = sorted(range(count), key=lambda j: (abs(j - here), j))[k]
        place = place + jnp.where(me == here, there, 0).astype(jnp.int32)
    return place


def make_kernel(sp, dp, xs, ys, parts, tok, width, taps, rows, cols, pad):
    group = sp // parts
    part_cols = group * cols
    half_rows = rows // 2
    blocks = width // LANES
    row_chunk = 128 if tok % 128 == 0 else tok
    lead = pad - (taps - 1)
    in_parts = 4 if blocks % 4 == 0 else 1
    in_cols = width // in_parts
    streamed = rows % LANES == 0

    def kernel(v_hbm, g_hbm, taps_hbm, gain_hbm, shift_hbm, w_hbm, out_hbm,
               v_in, g_in, halo_v, halo_g, taps_in, taps_f, gain, shift, gated, conv, act, acc, out_v, wall,
               in_sem, out_sem, halo_send, halo_recv, send_sem, z_sem, recv_sem):
        s = lax.axis_index("sp")
        d = lax.axis_index("dp")
        core = lax.rem(d, 2)
        x = lax.rem(d // 2, xs)
        y = d // (2 * xs)

        def index(yy, xx, cc):
            return (yy * xs + xx) * 2 + cc

        sibling = index(y, x, 1 - core)

        def along_x(step):
            return lax.rem(x + step, xs)

        def along_y(step):
            return lax.rem(y + step, ys)

        own = wall.at[pl.ds(pl.multiple_of(d * rows, rows), rows), pl.ds(pl.multiple_of(s * cols, cols), cols)]
        w_copy = pltpu.make_async_copy(w_hbm, own, in_sem.at[0])
        w_copy.start()
        loads = []
        for part in range(in_parts):
            sl = pl.ds(part * in_cols, in_cols)
            pair = (
                pltpu.make_async_copy(v_hbm.at[0, :, sl], v_in.at[:, sl], in_sem.at[4 + 2 * part]),
                pltpu.make_async_copy(g_hbm.at[0, :, sl], g_in.at[:, sl], in_sem.at[5 + 2 * part]),
            )
            loads.append(pair)
            for copy in pair:
                copy.start()
        small = [
            pltpu.make_async_copy(taps_hbm, taps_in, in_sem.at[1]),
            pltpu.make_async_copy(gain_hbm, gain, in_sem.at[2]),
            pltpu.make_async_copy(shift_hbm, shift, in_sem.at[3]),
        ]
        for copy in small:
            copy.start()

        barrier = pltpu.get_barrier_semaphore()
        friends = [(s, sibling)]
        friends += [(s, index(y, along_x(i), core)) for i in range(1, xs)]
        friends += [(s, index(along_y(i), x, core)) for i in range(1, ys)]
        friends += [(lax.rem(s + i, sp), d) for i in range(1, sp)]
        for friend in friends:
            pl.semaphore_signal(barrier, inc=1, device_id=friend, device_id_type=MESH)
        pl.semaphore_wait(barrier, len(friends))
        w_copy.wait()

        sent = []

        def send(region, sem, target):
            copy = pltpu.make_async_remote_copy(
                src_ref=region, dst_ref=region, send_sem=send_sem.at[len(sent)], recv_sem=sem,
                device_id=target, device_id_type=MESH)
            copy.start()
            sent.append(copy)

        def arrived(region, sem):
            pltpu.make_async_remote_copy(
                src_ref=region, dst_ref=region, send_sem=send_sem.at[0], recv_sem=sem,
                device_id=(s, sibling), device_id_type=MESH).wait_recv()

        def block(half, who):
            return wall.at[pl.ds(pl.multiple_of(d * rows + half * half_rows, half_rows), half_rows),
                           pl.ds(pl.multiple_of(who * cols, cols), cols)]

        def strip(half, dd, part):
            return wall.at[pl.ds(pl.multiple_of(dd * rows + half * half_rows, half_rows), half_rows),
                           pl.ds(pl.multiple_of(part * part_cols, part_cols), part_cols)]

        halo = [
            pltpu.make_async_remote_copy(
                src_ref=src.at[0, pl.ds(tok - pad, pad), :], dst_ref=dst, send_sem=halo_send.at[i],
                recv_sem=halo_recv.at[i], device_id=(lax.rem(s + 1, sp), d), device_id_type=MESH)
            for i, (src, dst) in enumerate(((v_hbm, halo_v), (g_hbm, halo_g)))
        ]

        def send_halo():
            @pl.when(s < sp - 1)
            def _():
                for copy in halo:
                    copy.start()

        def z_sends(first, last):
            for k in range(first, last):
                target = nearest(s, sp, k)
                for half in range(2):
                    send(block(half, s), z_sem.at[half, s], (s, d) if sp == 1 else (target, d))

        my_part = s // group
        part_of = [nearest(my_part, parts, k) for k in range(parts)]

        def firsts(half):
            if half == 0:
                return [index(y, along_x(i), core) for i in range(1, xs)]
            return [index(along_y(i), x, core) for i in range(1, ys)]

        def event_own(c):
            part = part_of[c]
            for half in range(2):
                for i in range(group):
                    who = part * group + i
                    if c == 0:
                        if group > 1:
                            @pl.when(who != s)
                            def _():
                                arrived(block(half, who), z_sem.at[half, who])
                    else:
                        arrived(block(half, who), z_sem.at[half, who])
                for target in firsts(half):
                    send(strip(half, d, part), recv_sem.at[half, d, part], (s, target))
            for half in range(2):
                for target in firsts(1 - half):
                    send(strip(half, d, part), recv_sem.at[half, d, part], (s, target))
            for half in range(2):
                send(strip(half, d, part), recv_sem.at[half, d, part], (s, sibling))

        def event_first(c):
            part = part_of[c]
            for half in (1, 0):
                for dd in firsts(half):
                    region, sem = strip(half, dd, part), recv_sem.at[half, dd, part]
                    arrived(region, sem)
                    for target in firsts(1 - half):
                        send(region, sem, (s, target))
                    send(region, sem, (s, sibling))

        def event_second(c):
            part = part_of[c]
            for first in range(max(xs, ys)):
                for second in range(1, max(xs, ys)):
                    for half in range(2):
                        fx, fy = (first, second) if half == 0 else (second, first)
                        if fx >= xs or fy >= ys:
                            continue
                        dd = index(along_y(fy), along_x(fx), core)
                        region, sem = strip(half, dd, part), recv_sem.at[half, dd, part]
                        arrived(region, sem)
                        send(region, sem, (s, sibling))

        def gated_rows(part):
            for copy in loads[part]:
                copy.wait()

            def body(j, carry):
                cs = pl.ds(pl.multiple_of(part * in_cols + j * LANES, LANES), LANES)
                value = v_in[:, cs].astype(F32)
                gate = g_in[:, cs].astype(F32)
                gated[pl.ds(pad, tok), cs] = (value * half_sigmoid(gate)).astype(BF16).astype(F32)
                return carry

            lax.fori_loop(0, in_cols // LANES, body, 0)

        def taps_up():
            for copy in small:
                copy.wait()
            taps_f[...] = taps_in[...].astype(F32)

        def halo_rows():
            @pl.when(s == 0)
            def _():
                gated[pl.ds(0, pad), :] = jnp.zeros((pad, width), F32)

            @pl.when(s > 0)
            def _():
                for copy in halo:
                    copy.wait_recv()

                def body(j, carry):
                    cs = pl.ds(pl.multiple_of(j * LANES, LANES), LANES)
                    value = halo_v[:, cs].astype(F32)
                    gate = halo_g[:, cs].astype(F32)
                    gated[pl.ds(0, pad), cs] = (value * half_sigmoid(gate)).astype(BF16).astype(F32)
                    return carry

                lax.fori_loop(0, blocks, body, 0)

        def mix(row_starts, lo, hi):
            def body(j, carry):
                cs = pl.ds(pl.multiple_of(j * LANES, LANES), LANES)
                for start in row_starts:
                    seen = gated[pl.ds(start, row_chunk + pad), cs]
                    total = None
                    for r in range(8):
                        inner = None
                        length = row_chunk + (8 if r else 0)
                        for q in range(0, pad // 8 + 1):
                            tap = 8 * q + r - lead
                            if 0 <= tap < taps:
                                term = seen[8 * q:8 * q + length] * taps_f[pl.ds(tap, 1), cs]
                                inner = term if inner is None else inner + term
                        if inner is None:
                            continue
                        if r:
                            inner = pltpu.roll(inner, length - r, 0)[:row_chunk]
                        total = inner if total is None else total + inner
                    conv[pl.ds(start, row_chunk), cs] = total.astype(BF16).astype(F32)
                return carry

            lax.fori_loop(lo, hi, body, 0)

        def normalise():
            step = 32 if tok % 32 == 0 else tok

            def body(i, carry):
                rs = pl.ds(pl.multiple_of(i * step, step), step)
                wide = conv[rs, :]
                mean = jnp.sum(wide, axis=1, keepdims=True) * (1.0 / width)
                centered = wide - mean
                variance = jnp.sum(centered * centered, axis=1, keepdims=True) * (1.0 / width)
                scale = lax.rsqrt(variance + EPSILON)
                normed = centered * scale * gain[...] + shift[...]
                act[rs, :] = (normed * half_sigmoid(normed)).astype(BF16)
                return carry

            lax.fori_loop(0, tok // step, body, 0)

        def product(dd, part):
            ks = pl.ds(pl.multiple_of(dd * rows, rows), rows)
            ns = pl.ds(pl.multiple_of(part * part_cols, part_cols), part_cols)
            return ns, jnp.dot(act[:, ks], wall[ks, ns], preferred_element_type=F32)

        def sibling_strip(dd, part):
            for half in range(2):
                arrived(strip(half, dd, part), recv_sem.at[half, dd, part])

        def mm_own(c):
            part = part_of[c]
            sibling_strip(sibling, part)
            if streamed:
                ns, first = product(d, part)
                acc[:, ns] = first
                ns, second = product(sibling, part)
                acc[:, ns] += second

        def mm_rest(c):
            part = part_of[c]

            def body(j, carry):
                xx = lax.rem(x + lax.rem(j, xs), xs)
                yy = lax.rem(y + j // xs, ys)
                theirs = index(yy, xx, 1 - core)
                if streamed:
                    ns, first = product(index(yy, xx, core), part)
                    acc[:, ns] += first
                sibling_strip(theirs, part)
                if streamed:
                    ns, second = product(theirs, part)
                    acc[:, ns] += second
                return carry

            lax.fori_loop(1, xs * ys, body, 0)
            if streamed:
                ns = pl.ds(pl.multiple_of(part * part_cols, part_cols), part_cols)
                out_v[:, ns] = acc[:, ns].astype(BF16)
                copy = pltpu.make_async_copy(out_v.at[:, ns], out_hbm.at[0, :, ns], out_sem.at[c])
                copy.start()
                outs.append(copy)

        outs = []
        early = [start for start in range(0, tok, row_chunk) if start >= pad]
        late = [start for start in range(0, tok, row_chunk) if start < pad]

        compute = [lambda p=p: gated_rows(p) for p in range(in_parts)] + [taps_up]
        quarter = max(1, blocks // 4)
        edges = list(range(0, blocks, quarter)) + [blocks]
        compute += [lambda a=a, b=b: mix(early, a, b) for a, b in zip(edges[:-1], edges[1:])]
        compute += [halo_rows, lambda: mix(late, 0, blocks), normalise]
        events = []
        for c in range(parts + 2):
            if 1 <= c < parts:
                events.append(lambda c=c: event_own(c))
            if 1 <= c <= parts:
                events.append(lambda c=c: event_first(c - 1))
            if c >= 2:
                events.append(lambda c=c: event_second(c - 2))

        z_sends(1, 2)
        event_own(0)
        send_halo()
        z_sends(2, sp)

        relays = []
        for c in range(parts):
            relays.append(("first", c))
            if c + 1 < parts:
                relays.append(("own", c + 1))
            if c >= 1:
                relays.append(("second", c - 1))
        relays.append(("second", parts - 1))
        run = {"own": event_own, "first": event_first, "second": event_second}
        between = {6: 1, 7: 1, 9: 1, 11: 1}
        done = 0
        for number, piece in enumerate(compute):
            piece()
            for _ in range(between.get(number, 0)):
                if done < len(relays):
                    run[relays[done][0]](relays[done][1])
                    done += 1
        pending = [("own", 0)] + relays
        for number, (kind, c) in enumerate(pending):
            if number > done:
                run[kind](c)
            if kind == "own":
                mm_own(c)
            if kind == "second":
                mm_rest(c)

        if not streamed:
            k_step = 2 * LANES
            n_step = 4 * LANES

            def body(i, carry):
                ns = pl.ds(pl.multiple_of(i * n_step, n_step), n_step)
                acc[:, ns] = jnp.zeros((tok, n_step), F32)

                def inner(k, carry):
                    ks = pl.ds(pl.multiple_of(k * k_step, k_step), k_step)
                    acc[:, ns] += jnp.dot(act[:, ks], wall[ks, ns], preferred_element_type=F32)
                    return carry

                lax.fori_loop(0, width // k_step, inner, 0)
                out_v[:, ns] = acc[:, ns].astype(BF16)
                return carry

            lax.fori_loop(0, width // n_step, body, 0)
            copy = pltpu.make_async_copy(out_v, out_hbm.at[0], out_sem.at[0])
            copy.start()
            outs.append(copy)

        for copy in outs:
            copy.wait()
        for copy in sent:
            copy.wait_send()

        @pl.when(s < sp - 1)
        def _():
            for copy in halo:
                copy.wait_send()

    per_half = [(xs, ys), (ys, xs)]
    sends = 2 * (sp - 1)
    for one, two in per_half:
        sends += parts * (one + two - 1) + parts * (one - 1) * two + parts * one * (two - 1)
    scratch = [
        pltpu.VMEM((tok, width), BF16),
        pltpu.VMEM((tok, width), BF16),
        pltpu.VMEM((pad, width), BF16),
        pltpu.VMEM((pad, width), BF16),
        pltpu.VMEM((taps, width), BF16),
        pltpu.VMEM((taps, width), F32),
        pltpu.VMEM((1, width), F32),
        pltpu.VMEM((1, width), F32),
        pltpu.VMEM((pad + tok, width), F32),
        pltpu.VMEM((tok, width), F32),
        pltpu.VMEM((tok, width), BF16),
        pltpu.VMEM((tok, width), F32),
        pltpu.VMEM((tok, width), BF16),
        pltpu.VMEM((dp * rows, sp * cols), BF16),
        pltpu.SemaphoreType.DMA((4 + 2 * in_parts,)),
        pltpu.SemaphoreType.DMA((parts,)),
        pltpu.SemaphoreType.DMA((2,)),
        pltpu.SemaphoreType.DMA((2,)),
        pltpu.SemaphoreType.DMA((sends,)),
        pltpu.SemaphoreType.DMA((2, sp)),
        pltpu.SemaphoreType.DMA((2, dp, parts)),
    ]
    return kernel, scratch


def solution(mesh):
    sp, dp = mesh.shape["sp"], mesh.shape["dp"]
    chips = dp // 2
    xs = max(i for i in range(1, math.isqrt(chips) + 1) if chips % i == 0)
    ys = chips // xs
    parts = math.gcd(sp, max(1, 32 // dp))

    def per_device(value_half, gate_half, conv_taps, norm_gain, norm_shift, out_weight):
        _, tok, width = value_half.shape
        taps = conv_taps.shape[0]
        rows, cols = out_weight.shape
        pad = -(-(taps - 1) // 16) * 16
        kernel, scratch = make_kernel(sp, dp, xs, ys, parts, tok, width, taps, rows, cols, pad)
        return pl.pallas_call(
            kernel,
            out_shape=jax.ShapeDtypeStruct(value_half.shape, BF16),
            in_specs=[pl.BlockSpec(memory_space=pl.ANY)] * 6,
            out_specs=pl.BlockSpec(memory_space=pl.ANY),
            scratch_shapes=scratch,
            compiler_params=pltpu.CompilerParams(
                collective_id=0, has_side_effects=True, vmem_limit_bytes=48 * 1024 * 1024),
        )(value_half, gate_half, conv_taps, norm_gain[None], norm_shift[None], out_weight)

    placed = (P("dp", "sp", None), P("dp", "sp", None), P(), P(), P(), P("dp", "sp"))
    return jax.shard_map(
        per_device, mesh=mesh, in_specs=placed, out_specs=P("dp", "sp", None), check_vma=False
    )
```

time: 111 us -> 66.7 us (0.60); the launches traced: 109 us -> 66.4 us
  waiting for transfers between devices: 66.9 us -> 0 us
  Pallas kernels: 0 us -> 59.2 us
  other arithmetic: 17.8 us -> 0 us
  between operations: 13.5 us -> 0.02 us
  matrix products: 8.49 us -> 0 us
  local copies, waits for them, and re-layouts: 0.05 us -> 7.21 us
  starting transfers between devices: 2.56 us -> 0 us
    all_gather x2 -> x0, waiting for transfers between devices: 63.2 us -> none  [the longest x1 33.6 us: per_device(): lax.all_gather(row_block, 'dp', axis=0, tiled=True)]
    pallas_call x0 -> x1, Pallas kernels: none -> 59.2 us  [per_device(): pl.pallas_call(kernel, out_shape=jax.ShapeDtypeStruct(value_half.shape, B...]
    reduce_sum x2 -> x0, other arithmetic: 14.8 us -> none  [the longest x1 14.3 us: per_device(): mean_row = jnp.mean(widened, axis=-1, keepdims=True)]
    dot_general x1 -> x0, matrix products: 8.49 us -> none  [per_device(): jnp.dot(activated, lax.all_gather(row_block, 'dp', axis=0, tiled=True), p...]
    unnamed x6 -> x13, local copies, waits for them, and re-layouts: 0.02 us -> 7.21 us
    ppermute x1 -> x0, waiting for transfers between devices: 2.98 us -> none  [passed_along(): lax.ppermute(value, axis, [(source, source + steps) for source in range(i...]
    convert_element_type x1 -> x0, other arithmetic: 2.79 us -> none  [per_device(): gated = (value_half[0].astype(jnp.float32) * jax.nn.sigmoid(gate_half[0]....]
    ppermute x1 -> x0, starting transfers between devices: 2.52 us -> none  [passed_along(): lax.ppermute(value, axis, [(source, source + steps) for source in range(i...]
  transfers between devices with their start and end apart: 3 -> 0, of which waited for: 3 -> 0; matrix products, arithmetic and copies ran while one was open for 16% -> 0% of each run, Pallas kernels for 0% -> 0%
where the time goes in v1:
time: 66.7 us; the launch traced here: 66.4 us
  Pallas kernels  59.2 us (89%)
  local copies, waits for them, and re-layouts  7.21 us (11%)
    pallas_call x1, Pallas kernels, per_device(): pl.pallas_call(kernel, out_shape=jax.ShapeDtypeStruct(value_half.shape, B...  59.2 us
    unnamed x13, local copies, waits for them, and re-layouts  7.21 us

profile of v1, /device:TPU:17, one launch (start us, length us, event | category | flops | bytes accessed | tf_op | source)
XLA Modules:
  0.0 66.4 jit_solution(13213482896011942032)
XLA Ops:
  0.0 0.0 copy-start
  0.0 1.4 %copy-done = bf16[1,384,2048]{2,1,0:T(8,128)(2,1)S(1)} copy-done((bf16[1,384,2048]{2,1,0:T(8,128)(2,1)S(1)}, bf16[1,384,2048]{2,1,0:T(8,128)(2,1)}, u32[]{:S(2)}) %copy-start) | copy-done | bytes 1572888
  1.4 0.0 copy-start.1
  1.4 1.4 %copy-done.1 = bf16[1,384,2048]{2,1,0:T(8,128)(2,1)S(1)} copy-done((bf16[1,384,2048]{2,1,0:T(8,128)(2,1)S(1)}, bf16[1,384,2048]{2,1,0:T(8,128)(2,1)}, u32[]{:S(2)}) %copy-start.1) | copy-done | bytes 1572888
  2.8 0.0 copy-start.2
  2.8 0.9 %copy-done.2 = bf16[256,512]{1,0:T(8,128)(2,1)S(1)} copy-done((bf16[256,512]{1,0:T(8,128)(2,1)S(1)}, bf16[256,512]{1,0:T(8,128)(2,1)}, u32[]{:S(2)}) %copy-start.2) | copy-done | bytes 262168
  3.8 0.0 copy-start.3
  3.8 0.9 %copy-done.3 = bf16[31,2048]{1,0:T(8,128)(2,1)S(1)} copy-done((bf16[31,2048]{1,0:T(8,128)(2,1)S(1)}, bf16[31,2048]{1,0:T(8,128)(2,1)}, u32[]{:S(2)}) %copy-start.3) | copy-done | bytes 127000
  4.7 0.0 copy-start.4
  4.7 0.7 %copy-done.4 = f32[2048]{0:T(1024)S(1)} copy-done((f32[2048]{0:T(1024)S(1)}, f32[2048]{0:T(1024)}, u32[]{:S(2)}) %copy-start.4) | copy-done | bytes 8216
  5.4 0.0 copy-start.5
  5.4 0.7 %copy-done.5 = f32[2048]{0:T(1024)S(1)} copy-done((f32[2048]{0:T(1024)S(1)}, f32[2048]{0:T(1024)}, u32[]{:S(2)}) %copy-start.5) | copy-done | bytes 8216
  6.1 59.2 %shard_map.64 = bf16[1,384,2048]{2,1,0:T(8,128)(2,1)S(1)} custom-call(bf16[1,384,2048]{2,1,0:T(8,128)(2,1)S(1)} %copy-done, bf16[1,384,2048]{2,1,0:T(8,128)(2,1)S(1)} %copy-done.1, bf16[31,2048]{1,0:T(8,128)(2,1)S(1)} %copy-done.3, f32[1,2048]{1,0:T(1,128)S(1)} %bitcast.2, f32[1,2048]{1,0:T(1,128)S(1)} %bitcast.3, bf16[256,512]{1,0:T(8,128)(2,1)S(1)} %copy-done.2), custom_call_target="tpu_custom_call" | custom-call | tf_op jit(solution)/shard_map/pallas_call | solution.py:426
  65.2 1.1 %copy.8 = bf16[1,384,2048]{2,1,0:T(8,128)(2,1)} copy(bf16[1,384,2048]{2,1,0:T(8,128)(2,1)S(1)} %shard_map.64) | data formatting | bytes 3145728
Async XLA Ops:
  0.0 1.4 %copy-start = (bf16[1,384,2048]{2,1,0:T(8,128)(2,1)S(1)}, bf16[1,384,2048]{2,1,0:T(8,128)(2,1)}, u32[]{:S(2)}) copy-start(bf16[1,384,2048]{2,1,0:T(8,128)(2,1)} %v_hbm.1) | copy-start | bytes 4718596
  1.4 1.4 %copy-start.1 = (bf16[1,384,2048]{2,1,0:T(8,128)(2,1)S(1)}, bf16[1,384,2048]{2,1,0:T(8,128)(2,1)}, u32[]{:S(2)}) copy-start(bf16[1,384,2048]{2,1,0:T(8,128)(2,1)} %g_hbm.1) | copy-start | bytes 4718596
  2.8 0.9 %copy-start.2 = (bf16[256,512]{1,0:T(8,128)(2,1)S(1)}, bf16[256,512]{1,0:T(8,128)(2,1)}, u32[]{:S(2)}) copy-start(bf16[256,512]{1,0:T(8,128)(2,1)} %w_hbm.1) | copy-start | bytes 786436
  3.8 0.9 %copy-start.3 = (bf16[31,2048]{1,0:T(8,128)(2,1)S(1)}, bf16[31,2048]{1,0:T(8,128)(2,1)}, u32[]{:S(2)}) copy-start(bf16[31,2048]{1,0:T(8,128)(2,1)} %taps_hbm.1) | copy-start | bytes 380932
  4.7 0.7 %copy-start.4 = (f32[2048]{0:T(1024)S(1)}, f32[2048]{0:T(1024)}, u32[]{:S(2)}) copy-start(f32[2048]{0:T(1024)} %param.9) | copy-start | bytes 24580
  5.4 0.7 %copy-start.5 = (f32[2048]{0:T(1024)S(1)}, f32[2048]{0:T(1024)}, u32[]{:S(2)}) copy-start(f32[2048]{0:T(1024)} %param.10) | copy-start | bytes 24580

commit v2 on v1

--- a/solution.py
+++ b/solution.py
@@ -12,6 +12,7 @@
 F32 = jnp.float32
 BF16 = jnp.bfloat16
 LANES = 128
+BEHIND = {6: 2, 7: 2, 8: 1, 10: 1, 11: 1, 12: 1}
 
 
 def half_sigmoid(x):
@@ -39,7 +40,7 @@
 
     def kernel(v_hbm, g_hbm, taps_hbm, gain_hbm, shift_hbm, w_hbm, out_hbm,
                v_in, g_in, halo_v, halo_g, taps_in, taps_f, gain, shift, gated, conv, act, acc, out_v, wall,
-               in_sem, out_sem, halo_send, halo_recv, send_sem, z_sem, recv_sem):
+               in_sem, out_sem, halo_send, halo_recv, send_sem, z_send, z_sem, recv_sem):
         s = lax.axis_index("sp")
         d = lax.axis_index("dp")
         core = lax.rem(d, 2)
@@ -123,11 +124,46 @@
                 for copy in halo:
                     copy.start()
 
-        def z_sends(first, last):
-            for k in range(first, last):
-                target = nearest(s, sp, k)
+        guarded = []
+
+        def send_if(wanted, region, sem, target):
+            copy = pltpu.make_async_remote_copy(
+                src_ref=region, dst_ref=region, send_sem=z_send.at[len(guarded)], recv_sem=sem,
+                device_id=(target, d), device_id_type=MESH)
+
+            @pl.when(wanted)
+            def _():
+                copy.start()
+
+            guarded.append((wanted, copy))
+
+        def z_sends():
+            for half in range(2):
+                send_if(s + 1 < sp, block(half, s), z_sem.at[half, s], lax.rem(s + 1, sp))
+                send_if(s > 0, block(half, s), z_sem.at[half, s], lax.rem(s + sp - 1, sp))
+
+        def z_link(k):
+            source = nearest(s, sp, k)
+            target = jnp.where(source < s, s + 1, s - 1)
+            onward = jnp.logical_and(target >= 0, target < sp)
+            return source, lax.rem(target + sp, sp), onward
+
+        def z_forward(k):
+            source, target, onward = z_link(k)
+            for half in range(2):
+                @pl.when(onward)
+                def _():
+                    arrived(block(half, source), z_sem.at[half, source])
+
+                send_if(onward, block(half, source), z_sem.at[half, source], target)
+
+        def z_last(k):
+            source, _, onward = z_link(k)
+
+            @pl.when(jnp.logical_not(onward))
+            def _():
                 for half in range(2):
-                    send(block(half, s), z_sem.at[half, s], (s, d) if sp == 1 else (target, d))
+                    arrived(block(half, source), z_sem.at[half, source])
 
         my_part = s // group
         part_of = [nearest(my_part, parts, k) for k in range(parts)]
@@ -139,16 +175,9 @@
 
         def event_own(c):
             part = part_of[c]
-            for half in range(2):
-                for i in range(group):
-                    who = part * group + i
-                    if c == 0:
-                        if group > 1:
-                            @pl.when(who != s)
-                            def _():
-                                arrived(block(half, who), z_sem.at[half, who])
-                    else:
-                        arrived(block(half, who), z_sem.at[half, who])
+            if group == 1 and c > 0:
+                z_last(c)
+            for half in range(2):
                 for target in firsts(half):
                     send(strip(half, d, part), recv_sem.at[half, d, part], (s, target))
             for half in range(2):
@@ -303,49 +332,48 @@
         early = [start for start in range(0, tok, row_chunk) if start >= pad]
         late = [start for start in range(0, tok, row_chunk) if start < pad]
 
-        compute = [lambda p=p: gated_rows(p) for p in range(in_parts)] + [taps_up]
         quarter = max(1, blocks // 4)
         edges = list(range(0, blocks, quarter)) + [blocks]
-        compute += [lambda a=a, b=b: mix(early, a, b) for a, b in zip(edges[:-1], edges[1:])]
-        compute += [halo_rows, lambda: mix(late, 0, blocks), normalise]
-        events = []
-        for c in range(parts + 2):
-            if 1 <= c < parts:
-                events.append(lambda c=c: event_own(c))
-            if 1 <= c <= parts:
-                events.append(lambda c=c: event_first(c - 1))
-            if c >= 2:
-                events.append(lambda c=c: event_second(c - 2))
-
-        z_sends(1, 2)
-        event_own(0)
-        send_halo()
-        z_sends(2, sp)
-
-        relays = []
-        for c in range(parts):
-            relays.append(("first", c))
-            if c + 1 < parts:
-                relays.append(("own", c + 1))
-            if c >= 1:
-                relays.append(("second", c - 1))
-        relays.append(("second", parts - 1))
-        run = {"own": event_own, "first": event_first, "second": event_second}
-        between = {6: 1, 7: 1, 9: 1, 11: 1}
+        mixes = list(zip(edges[:-1], edges[1:]))
+        plan = []
+        z_sends()
+        if group > 1:
+            send_halo()
+            for k in range(1, sp):
+                z_forward(k)
+                z_last(k)
+            event_own(0)
+        else:
+            event_own(0)
+            send_halo()
+        plan = [lambda p=p: gated_rows(p) for p in range(in_parts)] + [taps_up]
+        plan += [lambda a=a, b=b: mix(early, a, b) for a, b in mixes]
+        plan += [halo_rows]
+        plan += [lambda a=a, b=b: mix(late, a, b) for a, b in mixes]
+        plan += [normalise]
+        relays = ["z1", "f0", "o1", "z2", "z3", "f1", "o2", "s0", "f2", "o3", "s1", "f3", "s2", "s3"]
+        known = [name for name in relays if int(name[1:]) < (sp if name[0] == "z" else parts)]
+        known = [name for name in known if not (name[0] == "z" and group > 1)]
+        for k in range(4, sp if group == 1 else 0):
+            known.append("z%d" % k)
+        for c in range(4, parts):
+            known += ["o%d" % c, "f%d" % c, "s%d" % c]
+        run = {"z": z_forward, "o": event_own, "f": event_first, "s": event_second}
+        behind = BEHIND
         done = 0
-        for number, piece in enumerate(compute):
+        for number, piece in enumerate(plan):
             piece()
-            for _ in range(between.get(number, 0)):
-                if done < len(relays):
-                    run[relays[done][0]](relays[done][1])
+            for _ in range(behind.get(number, 0)):
+                if done < len(known):
+                    run[known[done][0]](int(known[done][1:]))
                     done += 1
-        pending = [("own", 0)] + relays
-        for number, (kind, c) in enumerate(pending):
+        for number, name in enumerate(["o0"] + known):
+            kind, c = name[0], int(name[1:])
             if number > done:
                 run[kind](c)
-            if kind == "own":
+            if kind == "o":
                 mm_own(c)
-            if kind == "second":
+            if kind == "s":
                 mm_rest(c)
 
         if not streamed:
@@ -375,13 +403,18 @@
         for copy in sent:
             copy.wait_send()
 
+        for wanted, copy in guarded:
+            @pl.when(wanted)
+            def _():
+                copy.wait_send()
+
         @pl.when(s < sp - 1)
         def _():
             for copy in halo:
                 copy.wait_send()
 
     per_half = [(xs, ys), (ys, xs)]
-    sends = 2 * (sp - 1)
+    sends = 0
     for one, two in per_half:
         sends += parts * (one + two - 1) + parts * (one - 1) * two + parts * one * (two - 1)
     scratch = [
@@ -404,6 +437,7 @@
         pltpu.SemaphoreType.DMA((2,)),
         pltpu.SemaphoreType.DMA((2,)),
         pltpu.SemaphoreType.DMA((sends,)),
+        pltpu.SemaphoreType.DMA((2 * (sp + 1),)),
         pltpu.SemaphoreType.DMA((2, sp)),
         pltpu.SemaphoreType.DMA((2, dp, parts)),
     ]
@@ -426,11 +460,11 @@
         return pl.pallas_call(
             kernel,
             out_shape=jax.ShapeDtypeStruct(value_half.shape, BF16),
-            in_specs=[pl.BlockSpec(memory_space=pl.ANY)] * 6,
-            out_specs=pl.BlockSpec(memory_space=pl.ANY),
+            in_specs=[pl.BlockSpec(memory_space=pltpu.HBM)] * 6,
+            out_specs=pl.BlockSpec(memory_space=pltpu.HBM),
             scratch_shapes=scratch,
             compiler_params=pltpu.CompilerParams(
-                collective_id=0, has_side_effects=True, vmem_limit_bytes=48 * 1024 * 1024),
+                collective_id=0, has_side_effects=True, vmem_limit_bytes=63 * 1024 * 1024),
         )(value_half, gate_half, conv_taps, norm_gain[None], norm_shift[None], out_weight)
 
     placed = (P("dp", "sp", None), P("dp", "sp", None), P(), P(), P(), P("dp", "sp"))

time: 66.7 us -> 49.6 us (0.74)
  Pallas kernels: 59.2 us -> 46.7 us
  local copies, waits for them, and re-layouts: 7.21 us -> 2.73 us
    pallas_call x1, Pallas kernels: 59.2 us -> 46.7 us  [per_device(): pl.pallas_call(kernel, out_shape=jax.ShapeDtypeStruct(value_half.shape, B...]
    unnamed x13 -> x1, local copies, waits for them, and re-layouts: 7.21 us -> 2.73 us
where the time goes in v2:
time: 49.6 us; the launch traced here: 49.5 us
  Pallas kernels  46.7 us (94%)
  local copies, waits for them, and re-layouts  2.73 us (6%)
    pallas_call x1, Pallas kernels, per_device(): pl.pallas_call(kernel, out_shape=jax.ShapeDtypeStruct(value_half.shape, B...  46.7 us
    unnamed x1, local copies, waits for them, and re-layouts  2.73 us

profile of v2, /device:TPU:17, one launch (start us, length us, event | category | flops | bytes accessed | tf_op | source)
XLA Modules:
  0.0 49.5 jit_solution(11030921200507731488)
XLA Ops:
  0.0 46.7 %shard_map.64 = bf16[1,384,2048]{2,1,0:T(8,128)(2,1)} custom-call(bf16[1,384,2048]{2,1,0:T(8,128)(2,1)} %v_hbm.1, bf16[1,384,2048]{2,1,0:T(8,128)(2,1)} %g_hbm.1, bf16[31,2048]{1,0:T(8,128)(2,1)} %taps_hbm.1, f32[1,2048]{1,0:T(1,128)} %bitcast.2, f32[1,2048]{1,0:T(1,128)} %bitcast.3, bf16[256,512]{1,0:T(8,128)(2,1)} %w_hbm.1), custom_call_target="tpu_custom_call" | custom-call | tf_op jit(solution)/shard_map/pallas_call | solution.py:460
  46.8 2.7 %copy.8 = bf16[1,384,2048]{2,1,0:T(8,128)(2,1)} copy(bf16[1,384,2048]{2,1,0:T(8,128)(2,1)} %shard_map.64) | data formatting | bytes 3145728

commit v3 on v2

--- a/solution.py
+++ b/solution.py
@@ -12,6 +12,7 @@
 F32 = jnp.float32
 BF16 = jnp.bfloat16
 LANES = 128
+VMEM_LIMIT = 62 * 1024 * 1024
 BEHIND = {6: 2, 7: 2, 8: 1, 10: 1, 11: 1, 12: 1}
 
 
@@ -38,9 +39,9 @@
     in_cols = width // in_parts
     streamed = rows % LANES == 0
 
-    def kernel(v_hbm, g_hbm, taps_hbm, gain_hbm, shift_hbm, w_hbm, out_hbm,
-               v_in, g_in, halo_v, halo_g, taps_in, taps_f, gain, shift, gated, conv, act, acc, out_v, wall,
-               in_sem, out_sem, halo_send, halo_recv, send_sem, z_send, z_sem, recv_sem):
+    def kernel(v_hbm, g_hbm, taps_hbm, gain_hbm, shift_hbm, w_hbm, out_v,
+               v_in, g_in, halo_v, halo_g, taps_in, taps_f, gain, shift, gated, conv, act, acc, wall,
+               in_sem, halo_send, halo_recv, send_sem, z_send, z_sem, recv_sem):
         s = lax.axis_index("sp")
         d = lax.axis_index("dp")
         core = lax.rem(d, 2)
@@ -323,12 +324,8 @@
             lax.fori_loop(1, xs * ys, body, 0)
             if streamed:
                 ns = pl.ds(pl.multiple_of(part * part_cols, part_cols), part_cols)
-                out_v[:, ns] = acc[:, ns].astype(BF16)
-                copy = pltpu.make_async_copy(out_v.at[:, ns], out_hbm.at[0, :, ns], out_sem.at[c])
-                copy.start()
-                outs.append(copy)
-
-        outs = []
+                out_v[0, :, ns] = acc[:, ns].astype(BF16)
+
         early = [start for start in range(0, tok, row_chunk) if start >= pad]
         late = [start for start in range(0, tok, row_chunk) if start < pad]
 
@@ -390,16 +387,11 @@
                     return carry
 
                 lax.fori_loop(0, width // k_step, inner, 0)
-                out_v[:, ns] = acc[:, ns].astype(BF16)
+                out_v[0, :, ns] = acc[:, ns].astype(BF16)
                 return carry
 
             lax.fori_loop(0, width // n_step, body, 0)
-            copy = pltpu.make_async_copy(out_v, out_hbm.at[0], out_sem.at[0])
-            copy.start()
-            outs.append(copy)
-
-        for copy in outs:
-            copy.wait()
+
         for copy in sent:
             copy.wait_send()
 
@@ -430,10 +422,8 @@
         pltpu.VMEM((tok, width), F32),
         pltpu.VMEM((tok, width), BF16),
         pltpu.VMEM((tok, width), F32),
-        pltpu.VMEM((tok, width), BF16),
         pltpu.VMEM((dp * rows, sp * cols), BF16),
         pltpu.SemaphoreType.DMA((4 + 2 * in_parts,)),
-        pltpu.SemaphoreType.DMA((parts,)),
         pltpu.SemaphoreType.DMA((2,)),
         pltpu.SemaphoreType.DMA((2,)),
         pltpu.SemaphoreType.DMA((sends,)),
@@ -459,12 +449,12 @@
         kernel, scratch = make_kernel(sp, dp, xs, ys, parts, tok, width, taps, rows, cols, pad)
         return pl.pallas_call(
             kernel,
-            out_shape=jax.ShapeDtypeStruct(value_half.shape, BF16),
+            out_shape=pltpu.VMEM(value_half.shape, BF16),
             in_specs=[pl.BlockSpec(memory_space=pltpu.HBM)] * 6,
-            out_specs=pl.BlockSpec(memory_space=pltpu.HBM),
+            out_specs=pl.BlockSpec(memory_space=pltpu.VMEM),
             scratch_shapes=scratch,
             compiler_params=pltpu.CompilerParams(
-                collective_id=0, has_side_effects=True, vmem_limit_bytes=63 * 1024 * 1024),
+                collective_id=0, has_side_effects=True, vmem_limit_bytes=VMEM_LIMIT),
         )(value_half, gate_half, conv_taps, norm_gain[None], norm_shift[None], out_weight)
 
     placed = (P("dp", "sp", None), P("dp", "sp", None), P(), P(), P(), P("dp", "sp"))

time: 49.6 us -> 47.2 us (0.952)
  local copies, waits for them, and re-layouts: 2.73 us -> 1.15 us
  Pallas kernels: 46.7 us -> 45.9 us
    unnamed x1, local copies, waits for them, and re-layouts: 2.73 us -> 1.15 us
    pallas_call x1, Pallas kernels: 46.7 us -> 45.9 us  [per_device(): pl.pallas_call(kernel, out_shape=pltpu.VMEM(value_half.shape, BF16), in_s...]
where the time goes in v3:
time: 47.2 us; the launch traced here: 47.1 us
  Pallas kernels  45.9 us (97%)
  local copies, waits for them, and re-layouts  1.15 us (2%)
    pallas_call x1, Pallas kernels, per_device(): pl.pallas_call(kernel, out_shape=pltpu.VMEM(value_half.shape, BF16), in_s...  45.9 us
    unnamed x1, local copies, waits for them, and re-layouts  1.15 us

profile of v3, /device:TPU:17, one launch (start us, length us, event | category | flops | bytes accessed | tf_op | source)
XLA Modules:
  0.0 47.1 jit_solution(13814499509315617560)
XLA Ops:
  0.0 45.9 %shard_map.64 = bf16[1,384,2048]{2,1,0:T(8,128)(2,1)S(1)} custom-call(bf16[1,384,2048]{2,1,0:T(8,128)(2,1)} %v_hbm.1, bf16[1,384,2048]{2,1,0:T(8,128)(2,1)} %g_hbm.1, bf16[31,2048]{1,0:T(8,128)(2,1)} %taps_hbm.1, f32[1,2048]{1,0:T(1,128)} %bitcast.2, f32[1,2048]{1,0:T(1,128)} %bitcast.3, bf16[256,512]{1,0:T(8,128)(2,1)} %w_hbm.1), custom_call_target="tpu_custom_call" | custom-call | tf_op jit(solution)/shard_map/pallas_call | solution.py:450
  45.9 1.1 %copy.8 = bf16[1,384,2048]{2,1,0:T(8,128)(2,1)} copy(bf16[1,384,2048]{2,1,0:T(8,128)(2,1)S(1)} %shard_map.64) | data formatting | bytes 3145728

commit v4 on v3

--- a/solution.py
+++ b/solution.py
@@ -13,7 +13,12 @@
 BF16 = jnp.bfloat16
 LANES = 128
 VMEM_LIMIT = 62 * 1024 * 1024
-BEHIND = {6: 2, 7: 2, 8: 1, 10: 1, 11: 1, 12: 1}
+ORDER = (
+    "x0", "g0", "g1", "g2", "g3", "t0", "e0", "f0", "e1", "z1", "a0", "o1",
+    "e2", "y0", "z2", "e3", "f1", "n0", "z3", "v0", "o2", "s0", "h0", "l0",
+    "l1", "l2", "l3", "f2", "n1", "o3", "w1", "w2", "u1", "m0", "r0", "s1",
+    "m1", "r1", "w3", "f3", "u2", "s2", "m2", "r2", "u3", "m3", "s3", "r3",
+)
 
 
 def half_sigmoid(x):
@@ -31,7 +36,9 @@
 def make_kernel(sp, dp, xs, ys, parts, tok, width, taps, rows, cols, pad):
     group = sp // parts
     part_cols = group * cols
-    half_rows = rows // 2
+    late_rows = rows // 8 // 16 * 16 if group == 1 else 0
+    half_rows = (rows - late_rows) // 2
+    chips = xs * ys
     blocks = width // LANES
     row_chunk = 128 if tok % 128 == 0 else tok
     lead = pad - (taps - 1)
@@ -41,7 +48,7 @@
 
     def kernel(v_hbm, g_hbm, taps_hbm, gain_hbm, shift_hbm, w_hbm, out_v,
                v_in, g_in, halo_v, halo_g, taps_in, taps_f, gain, shift, gated, conv, act, acc, wall,
-               in_sem, halo_send, halo_recv, send_sem, z_send, z_sem, recv_sem):
+               in_sem, halo_send, halo_recv, send_sem, z_send, z_sem, recv_sem, late_sem):
         s = lax.axis_index("sp")
         d = lax.axis_index("dp")
         core = lax.rem(d, 2)
@@ -105,11 +112,11 @@
                 device_id=(s, sibling), device_id_type=MESH).wait_recv()
 
         def block(half, who):
-            return wall.at[pl.ds(pl.multiple_of(d * rows + half * half_rows, half_rows), half_rows),
+            return wall.at[pl.ds(pl.multiple_of(d * rows + half * half_rows, 16), half_rows),
                            pl.ds(pl.multiple_of(who * cols, cols), cols)]
 
         def strip(half, dd, part):
-            return wall.at[pl.ds(pl.multiple_of(dd * rows + half * half_rows, half_rows), half_rows),
+            return wall.at[pl.ds(pl.multiple_of(dd * rows + half * half_rows, 16), half_rows),
                            pl.ds(pl.multiple_of(part * part_cols, part_cols), part_cols)]
 
         halo = [
@@ -119,18 +126,17 @@
             for i, (src, dst) in enumerate(((v_hbm, halo_v), (g_hbm, halo_g)))
         ]
 
-        def send_halo():
+        def send_halo(i):
             @pl.when(s < sp - 1)
             def _():
-                for copy in halo:
-                    copy.start()
+                halo[i].start()
 
         guarded = []
 
-        def send_if(wanted, region, sem, target):
+        def send_if(wanted, region, sem, target, column=None):
             copy = pltpu.make_async_remote_copy(
                 src_ref=region, dst_ref=region, send_sem=z_send.at[len(guarded)], recv_sem=sem,
-                device_id=(target, d), device_id_type=MESH)
+                device_id=(target, d if column is None else column), device_id_type=MESH)
 
             @pl.when(wanted)
             def _():
@@ -209,6 +215,60 @@
                         region, sem = strip(half, dd, part), recv_sem.at[half, dd, part]
                         arrived(region, sem)
                         send(region, sem, (s, sibling))
+
+        def late_strip(dd, who):
+            return wall.at[pl.ds(pl.multiple_of(dd * rows + 2 * half_rows, 16), late_rows),
+                           pl.ds(pl.multiple_of(who * cols, cols), cols)]
+
+        def mine(i):
+            return index(along_y(i // xs), along_x(i % xs), core)
+
+        def late_send(dd, target):
+            send(late_strip(dd, s), late_sem.at[dd, s], (s, target))
+
+        def late_x():
+            for i in range(1, xs):
+                late_send(d, mine(i))
+
+        def late_y():
+            for i in range(xs):
+                if i:
+                    arrived(late_strip(mine(i), s), late_sem.at[mine(i), s])
+                for j in range(1, ys):
+                    late_send(mine(i), index(along_y(j), x, core))
+
+        def late_z():
+            for i in range(chips):
+                dd = mine(i)
+                if i >= xs:
+                    arrived(late_strip(dd, s), late_sem.at[dd, s])
+                send_if(s + 1 < sp, late_strip(dd, s), late_sem.at[dd, s], lax.rem(s + 1, sp))
+                send_if(s > 0, late_strip(dd, s), late_sem.at[dd, s], lax.rem(s + sp - 1, sp))
+                late_send(dd, sibling)
+
+        def late_forward(k):
+            source, target, onward = z_link(k)
+            for i in range(chips):
+                region, sem = late_strip(mine(i), source), late_sem.at[mine(i), source]
+
+                @pl.when(onward)
+                def _():
+                    arrived(region, sem)
+
+                send_if(onward, region, sem, target)
+                send_if(onward, region, sem, s, sibling)
+
+        def late_last(k):
+            source, _, onward = z_link(k)
+            ended = jnp.logical_not(onward)
+            for i in range(chips):
+                region, sem = late_strip(mine(i), source), late_sem.at[mine(i), source]
+
+                @pl.when(ended)
+                def _():
+                    arrived(region, sem)
+
+                send_if(ended, region, sem, s, sibling)
 
         def gated_rows(part):
             for copy in loads[part]:
@@ -271,8 +331,8 @@
 
             lax.fori_loop(lo, hi, body, 0)
 
-        def normalise():
-            step = 32 if tok % 32 == 0 else tok
+        def normalise(low, high):
+            step = math.gcd(32, row_chunk)
 
             def body(i, carry):
                 rs = pl.ds(pl.multiple_of(i * step, step), step)
@@ -285,7 +345,7 @@
                 act[rs, :] = (normed * half_sigmoid(normed)).astype(BF16)
                 return carry
 
-            lax.fori_loop(0, tok // step, body, 0)
+            lax.fori_loop(low // step, high // step, body, 0)
 
         def product(dd, part):
             ks = pl.ds(pl.multiple_of(dd * rows, rows), rows)
@@ -295,6 +355,8 @@
         def sibling_strip(dd, part):
             for half in range(2):
                 arrived(strip(half, dd, part), recv_sem.at[half, dd, part])
+            if late_rows:
+                arrived(late_strip(dd, part), late_sem.at[dd, part])
 
         def mm_own(c):
             part = part_of[c]
@@ -329,49 +391,44 @@
         early = [start for start in range(0, tok, row_chunk) if start >= pad]
         late = [start for start in range(0, tok, row_chunk) if start < pad]
 
-        quarter = max(1, blocks // 4)
-        edges = list(range(0, blocks, quarter)) + [blocks]
-        mixes = list(zip(edges[:-1], edges[1:]))
-        plan = []
+        edges = [blocks * i // 4 for i in range(5)]
         z_sends()
         if group > 1:
-            send_halo()
+            send_halo(0)
             for k in range(1, sp):
                 z_forward(k)
                 z_last(k)
             event_own(0)
         else:
             event_own(0)
-            send_halo()
-        plan = [lambda p=p: gated_rows(p) for p in range(in_parts)] + [taps_up]
-        plan += [lambda a=a, b=b: mix(early, a, b) for a, b in mixes]
-        plan += [halo_rows]
-        plan += [lambda a=a, b=b: mix(late, a, b) for a, b in mixes]
-        plan += [normalise]
-        relays = ["z1", "f0", "o1", "z2", "z3", "f1", "o2", "s0", "f2", "o3", "s1", "f3", "s2", "s3"]
-        known = [name for name in relays if int(name[1:]) < (sp if name[0] == "z" else parts)]
-        known = [name for name in known if not (name[0] == "z" and group > 1)]
-        for k in range(4, sp if group == 1 else 0):
-            known.append("z%d" % k)
-        for c in range(4, parts):
-            known += ["o%d" % c, "f%d" % c, "s%d" % c]
-        run = {"z": z_forward, "o": event_own, "f": event_first, "s": event_second}
-        behind = BEHIND
-        done = 0
-        for number, piece in enumerate(plan):
-            piece()
-            for _ in range(behind.get(number, 0)):
-                if done < len(known):
-                    run[known[done][0]](int(known[done][1:]))
-                    done += 1
-        for number, name in enumerate(["o0"] + known):
-            kind, c = name[0], int(name[1:])
-            if number > done:
-                run[kind](c)
-            if kind == "o":
-                mm_own(c)
-            if kind == "s":
-                mm_rest(c)
+            send_halo(0)
+        run = {
+            "g": (gated_rows, 0, in_parts),
+            "t": (lambda c: taps_up(), 0, 1),
+            "e": (lambda c: mix(early, edges[c], edges[c + 1]), 0, 4),
+            "h": (lambda c: halo_rows(), 0, 1),
+            "l": (lambda c: mix(late, edges[c], edges[c + 1]), 0, 4),
+            "n": (lambda c: normalise(*((late[-1] + row_chunk, tok), (0, late[-1] + row_chunk))[c]), 0, 2),
+            "z": (z_forward, 1, sp if group == 1 else 0),
+            "o": (event_own, 1, parts),
+            "f": (event_first, 0, parts),
+            "s": (event_second, 0, parts),
+            "a": (lambda c: send_halo(1), 0, 1),
+            "x": (lambda c: late_x(), 0, 1 if late_rows else 0),
+            "y": (lambda c: late_y(), 0, 1 if late_rows else 0),
+            "v": (lambda c: late_z(), 0, 1 if late_rows else 0),
+            "w": (late_forward, 1, sp if late_rows else 0),
+            "u": (late_last, 1, sp if late_rows else 0),
+            "m": (mm_own, 0, parts),
+            "r": (mm_rest, 0, parts),
+        }
+        order = list(ORDER)
+        for c in range(max(sp, parts)):
+            order += [kind + str(c) for kind in "zowufsmr" if kind + str(c) not in order]
+        for name in order:
+            act_on, low, high = run[name[0]]
+            if low <= int(name[1:]) < high:
+                act_on(int(name[1:]))
 
         if not streamed:
             k_step = 2 * LANES
@@ -406,7 +463,7 @@
                 copy.wait_send()
 
     per_half = [(xs, ys), (ys, xs)]
-    sends = 0
+    sends = xs - 1 + xs * (ys - 1) + chips if late_rows else 0
     for one, two in per_half:
         sends += parts * (one + two - 1) + parts * (one - 1) * two + parts * one * (two - 1)
     scratch = [
@@ -427,9 +484,10 @@
         pltpu.SemaphoreType.DMA((2,)),
         pltpu.SemaphoreType.DMA((2,)),
         pltpu.SemaphoreType.DMA((sends,)),
-        pltpu.SemaphoreType.DMA((2 * (sp + 1),)),
+        pltpu.SemaphoreType.DMA((2 * (sp + 1) + chips * (3 * sp - 1),)),
         pltpu.SemaphoreType.DMA((2, sp)),
         pltpu.SemaphoreType.DMA((2, dp, parts)),
+        pltpu.SemaphoreType.DMA((dp, sp) if late_rows else (1, 1)),
     ]
     return kernel, scratch
 

time: 47.2 us -> 44.3 us (0.939)
  the two profiles are of different devices: /device:TPU:17 before, /device:TPU:1 now
where the time goes in v4:
time: 44.3 us; the launch traced here: 44.1 us
  Pallas kernels  43 us (97%)
  local copies, waits for them, and re-layouts  1.15 us (3%)
    pallas_call x1, Pallas kernels, per_device(): pl.pallas_call(kernel, out_shape=pltpu.VMEM(value_half.shape, BF16), in_s...  43 us
    unnamed x1, local copies, waits for them, and re-layouts  1.15 us

profile of v4, /device:TPU:1, one launch (start us, length us, event | category | flops | bytes accessed | tf_op | source)
XLA Modules:
  0.0 44.1 jit_solution(17738612351104027176)
XLA Ops:
  0.0 43.0 %shard_map.64 = bf16[1,384,2048]{2,1,0:T(8,128)(2,1)S(1)} custom-call(bf16[1,384,2048]{2,1,0:T(8,128)(2,1)} %v_hbm.1, bf16[1,384,2048]{2,1,0:T(8,128)(2,1)} %g_hbm.1, bf16[31,2048]{1,0:T(8,128)(2,1)} %taps_hbm.1, f32[1,2048]{1,0:T(1,128)} %bitcast.2, f32[1,2048]{1,0:T(1,128)} %bitcast.3, bf16[256,512]{1,0:T(8,128)(2,1)} %w_hbm.1), custom_call_target="tpu_custom_call" | custom-call | tf_op jit(solution)/shard_map/pallas_call | solution.py:508
  43.0 1.1 %copy.8 = bf16[1,384,2048]{2,1,0:T(8,128)(2,1)} copy(bf16[1,384,2048]{2,1,0:T(8,128)(2,1)S(1)} %shard_map.64) | data formatting | bytes 3145728
